TPU v7x, 32 devices: a whole 2x2x4 slice. The times are simulated.
32 devices in a mesh: grp: 2 (over y), sp: 4 (over z), tp: 4 (over x, core).
Axes of the slice: x: 2, y: 2, z: 4, core: 2. Of those that a mesh axis runs over, the one named last changes fastest.
Arguments:
- recurrent_query: bfloat16 [2048, 1024], P(('grp', 'sp'), 'tp'), parts along dimension 0, may hold values from -6 to 6
- recurrent_forget_gate: bfloat16 [2048, 1024], P(('grp', 'sp'), 'tp'), parts along dimension 0, may hold values from -4.5 to 4.5
- recurrent_value: bfloat16 [2048, 1024], P(('grp', 'sp'), 'tp'), parts along dimension 0, may hold values from -6 to 6
- recurrent_gate_lower_bound: float32 [1024], P('tp'), may hold values from 1.5 to 14
- recurrent_added_decay: float32 [2048, 8], P(('grp', 'sp'), 'tp'), parts along dimension 0, may hold values from -0.51 to 0
- recurrent_norm_gain: float32 [128], replicated, may hold values from 0.1 to 1.9
- attention_query_first: bfloat16 [2048, 512], P(('grp', 'sp'), 'tp'), parts along dimension 0, may hold values from -20 to 20
- attention_key_first: bfloat16 [2048, 256], P(('grp', 'sp'), 'tp'), parts along dimension 0, may hold values from -20 to 20
- attention_query_second: bfloat16 [2048, 512], P(('grp', 'sp'), 'tp'), parts along dimension 0, may hold values from -20 to 20
- attention_key_second: bfloat16 [2048, 256], P(('grp', 'sp'), 'tp'), parts along dimension 0, may hold values from -20 to 20
- attention_value: bfloat16 [2048, 512], P(('grp', 'sp'), 'tp'), parts along dimension 0, may hold values from -6 to 6
- second_map_weight: float32 [8], P('tp'), may hold values from 0.3 to 0.8
- attention_norm_gain: float32 [128], replicated, may hold values from 0.1 to 1.9
- output_weight: bfloat16 [2, 1024, 2048], P(None, 'tp', 'sp'), may hold values from -0.125 to 0.125
Outputs:
- mixed: bfloat16 [2048, 2048], P(('grp', 'sp', 'tp')), parts along dimension 0
There are 2 independent parts, one for each index of `grp`. A program takes and returns all parts, laid end to end along the dimension named above; an argument that names none is the same for every part. Nothing has to cross between parts.
All inputs are finite; a program needn't handle non-finite values.
Results may differ from a plain program's by a relative error of at most 0.02.
Values may be sent and summed in bfloat16 or wider, within the bound.
A program may use at most 64 MiB of HBM per device.

v0:
```python
import jax
import jax.numpy as jnp
from jax import lax
from jax.sharding import PartitionSpec as P

HG_DK = 128
HG_DV = 128
DA_HD = 64
BLK = 32


epsilon = 1e-06
highest = lax.Precision.HIGHEST
key_span = 512


def carried_in(array, axis, combine, identity):
    size, place = (lax.axis_size(axis), lax.axis_index(axis))
    everything = jax.tree.map(
        lambda part, kind: lax.all_gather(part.astype(kind), axis),
        array,
        (jnp.bfloat16, jnp.bfloat16),
    )
    start = jax.tree.map(
        lambda part, zero: jnp.broadcast_to(jnp.asarray(zero, part.dtype), part.shape),
        array,
        identity,
    )

    def hop(k, before):
        reached = k < place
        new = combine(
            before, jax.tree.map(lambda part, own: part[k].astype(own.dtype), everything, array)
        )
        return jax.tree.map(lambda a, b: jnp.where(reached, a, b), new, before)

    return lax.fori_loop(0, size, hop, start)


def head_norm(head_values, gain_vec):
    mean_square = jnp.mean(head_values * head_values, axis=-1, keepdims=True)
    return head_values * lax.rsqrt(mean_square + epsilon) * gain_vec


def decay_factors(gate_preactivation, lower_bound_logit, added_log_decay, number_of_heads):
    token_count = gate_preactivation.shape[0]
    floor_rate = jax.nn.sigmoid(-lower_bound_logit).reshape(number_of_heads, -1)
    state_inflow = floor_rate[None] * jax.nn.sigmoid(
        -gate_preactivation.astype(jnp.float32)
    ).reshape(token_count, number_of_heads, -1)
    decay_logarithm = jnp.log1p(-state_inflow) + added_log_decay[:, :, None]
    return (state_inflow, decay_logarithm)


def recurrence_blocks(queries, decay_logarithm, state_inflow, value_rows, block_len):
    token_count, number_of_heads, key_width = queries.shape
    block_count = token_count // block_len

    def to_blocks(source):
        return source.reshape(block_count, block_len, number_of_heads, source.shape[-1])

    causal = jnp.tril(jnp.ones((block_len, block_len), jnp.float32))[:, :, None, None]

    def block_step(carry_state, inputs):
        query_blk, decay_blk, inflow_blk, value_blk = inputs
        cumulative = jnp.cumsum(decay_blk, axis=0)
        relative = cumulative[:, None] - cumulative[None, :]
        decay_table = jnp.exp(jnp.minimum(relative, 0.0)) * causal
        scores = jnp.einsum(
            "thd,shd,tshd->hts", query_blk, inflow_blk, decay_table, precision=highest
        )
        block_out = jnp.einsum("hts,shv->thv", scores, value_blk, precision=highest)
        block_out = block_out + jnp.einsum(
            "thd,hdv->thv", query_blk * jnp.exp(cumulative), carry_state, precision=highest
        )
        last_log = cumulative[-1]
        new_state = jnp.exp(last_log)[:, :, None] * carry_state + jnp.einsum(
            "shd,shv->hdv",
            inflow_blk * jnp.exp(last_log[None] - cumulative),
            value_blk,
            precision=highest,
        )
        return (new_state, block_out)

    zero_state = jnp.zeros((number_of_heads, key_width, value_rows.shape[-1]), jnp.float32)
    final_state, outputs = lax.scan(
        block_step,
        zero_state,
        (
            to_blocks(queries),
            to_blocks(decay_logarithm),
            to_blocks(state_inflow),
            to_blocks(value_rows),
        ),
    )
    return (final_state, outputs.reshape(token_count, number_of_heads, -1))


def chain_pair(earlier, following):
    return (earlier[0] * following[0], following[0][:, :, None] * earlier[1] + following[1])


def recurrent_path_output(
    recurrent_query,
    recurrent_forget_gate,
    recurrent_value,
    recurrent_gate_lower_bound,
    recurrent_added_decay,
    recurrent_norm_gain,
):
    token_count = recurrent_query.shape[0]
    number_of_heads = recurrent_gate_lower_bound.shape[0] // HG_DK
    state_inflow, decay_logarithm = decay_factors(
        recurrent_forget_gate, recurrent_gate_lower_bound, recurrent_added_decay, number_of_heads
    )
    queries = recurrent_query.astype(jnp.float32).reshape(token_count, number_of_heads, HG_DK)
    value_rows = recurrent_value.astype(jnp.float32).reshape(token_count, number_of_heads, HG_DV)
    final_state, local_out = recurrence_blocks(
        queries, decay_logarithm, state_inflow, value_rows, BLK
    )
    running_log = jnp.cumsum(decay_logarithm, axis=0)
    through = jnp.exp(running_log[-1])
    incoming = carried_in(
        (through, final_state),
        "sp",
        chain_pair,
        (jnp.ones_like(through), jnp.zeros_like(final_state)),
    )
    carried = jnp.einsum(
        "thd,hdv->thv", queries * jnp.exp(running_log), incoming[1], precision=highest
    )
    return (
        head_norm(local_out + carried, recurrent_norm_gain)
        .astype(jnp.bfloat16)
        .reshape(token_count, -1)
    )


def attention_branch(
    attention_query_first,
    attention_key_first,
    attention_query_second,
    attention_key_second,
    attention_value,
    second_map_weight,
    attention_norm_gain,
):
    query_rows = attention_query_first.shape[0]
    key_heads = attention_key_first.shape[1] // DA_HD
    group_size = attention_query_first.shape[1] // DA_HD // key_heads
    score_scale = DA_HD ** (-0.5)
    offset = lax.axis_index("sp") * query_rows
    query_pos = offset + jnp.arange(query_rows)
    last_query = offset + query_rows - 1
    queries_one = attention_query_first.reshape(query_rows, key_heads, group_size, DA_HD)
    queries_two = attention_query_second.reshape(query_rows, key_heads, group_size, DA_HD)

    def map_update(running, queries, key_rows, value_rows, allowed):
        row_max, weight_mass, value_sum = running
        scores = (
            jnp.einsum("qkgd,skd->kgqs", queries, key_rows, preferred_element_type=jnp.float32)
            * score_scale
        )
        scores = jnp.where(allowed, scores, -1e30)
        new_max = jnp.maximum(row_max, jnp.max(scores, axis=-1))
        weights = jnp.where(allowed, jnp.exp(scores - new_max[..., None]), 0.0)
        shrink = jnp.exp(row_max - new_max)
        weight_mass = weight_mass * shrink + jnp.sum(weights, axis=-1)
        value_sum = value_sum * shrink[..., None] + jnp.einsum(
            "plew,wpd->pled",
            weights.astype(jnp.bfloat16),
            value_rows,
            preferred_element_type=jnp.float32,
        )
        return (new_max, weight_mass, value_sum)

    def key_block(running, block_one, block_two, block_values, first_row):
        span_rows = block_one.shape[0]
        key_pos = first_row + jnp.arange(span_rows)
        allowed = key_pos[None, :] <= query_pos[:, None]
        shaped_one = block_one.reshape(span_rows, key_heads, DA_HD)
        shaped_two = block_two.reshape(span_rows, key_heads, DA_HD)
        shaped_values = block_values.reshape(span_rows, key_heads, 2 * DA_HD)
        return (
            map_update(running[0], queries_one, shaped_one, shaped_values, allowed),
            map_update(running[1], queries_two, shaped_two, shaped_values, allowed),
        )

    def guarded_block(running, block_one, block_two, block_values, first_row):

        def compute(state_in):
            return key_block(state_in, block_one, block_two, block_values, first_row)

        def unchanged(state_in):
            return state_in

        result = lax.cond(first_row > last_query, unchanged, compute, running)
        return result

    start_max = jnp.full((key_heads, group_size, query_rows), -1e30, jnp.float32)
    zero_mass = jnp.zeros((key_heads, group_size, query_rows), jnp.float32)
    zero_sum = jnp.zeros((key_heads, group_size, query_rows, 2 * DA_HD), jnp.float32)
    fresh_state = (start_max, zero_mass, zero_sum)
    running = (fresh_state, fresh_state)
    shard_one = lax.all_gather(attention_key_first, "sp", axis=0, tiled=True)
    shard_two = lax.all_gather(attention_key_second, "sp", axis=0, tiled=True)
    shard_values = lax.all_gather(attention_value, "sp", axis=0, tiled=True)
    row_count = shard_one.shape[0]
    span_rows = min(row_count, key_span)
    full_count = row_count // span_rows

    def span_step(span_index, state_in):
        begin_row = span_index * span_rows
        return guarded_block(
            state_in,
            lax.dynamic_slice_in_dim(shard_one, begin_row, span_rows, 0),
            lax.dynamic_slice_in_dim(shard_two, begin_row, span_rows, 0),
            lax.dynamic_slice_in_dim(shard_values, begin_row, span_rows, 0),
            begin_row,
        )

    running = lax.fori_loop(0, full_count, span_step, running)
    first_map, second_map = running
    lambda_table = second_map_weight.reshape(key_heads, group_size)[:, :, None, None]
    combined = first_map[2] / first_map[1][..., None] - lambda_table * (
        second_map[2] / second_map[1][..., None]
    )
    combined = jnp.transpose(combined, (2, 0, 1, 3)).reshape(
        query_rows, key_heads * group_size, 2 * DA_HD
    )
    return head_norm(combined, attention_norm_gain).astype(jnp.bfloat16).reshape(query_rows, -1)


def shards(
    recurrent_query,
    recurrent_forget_gate,
    recurrent_value,
    recurrent_gate_lower_bound,
    recurrent_added_decay,
    recurrent_norm_gain,
    attention_query_first,
    attention_key_first,
    attention_query_second,
    attention_key_second,
    attention_value,
    second_map_weight,
    attention_norm_gain,
    output_weight,
):
    attended = attention_branch(
        attention_query_first,
        attention_key_first,
        attention_query_second,
        attention_key_second,
        attention_value,
        second_map_weight,
        attention_norm_gain,
    )
    recurrent_output = recurrent_path_output(
        recurrent_query,
        recurrent_forget_gate,
        recurrent_value,
        recurrent_gate_lower_bound,
        recurrent_added_decay,
        recurrent_norm_gain,
    )
    pieces = lax.all_gather(output_weight, "sp", axis=2, tiled=True)
    partial_terms = jnp.dot(
        recurrent_output, pieces[0], preferred_element_type=jnp.float32
    ) + jnp.dot(attended, pieces[1], preferred_element_type=jnp.float32)
    return lax.psum_scatter(
        partial_terms.astype(jnp.bfloat16), "tp", scatter_dimension=0, tiled=True
    )


def solution(mesh):
    return jax.shard_map(
        shards,
        mesh=mesh,
        in_specs=(
            P(("grp", "sp"), "tp"),
            P(("grp", "sp"), "tp"),
            P(("grp", "sp"), "tp"),
            P("tp"),
            P(("grp", "sp"), "tp"),
            P(),
            P(("grp", "sp"), "tp"),
            P(("grp", "sp"), "tp"),
            P(("grp", "sp"), "tp"),
            P(("grp", "sp"), "tp"),
            P(("grp", "sp"), "tp"),
            P("tp"),
            P(),
            P(None, "tp", "sp"),
        ),
        out_specs=P(("grp", "sp", "tp"), None),
        check_vma=False,
    )
```

profile of v0, /device:TPU:25, one launch (start us, length us, event | category | flops | bytes accessed | tf_op | source)
XLA Modules:
  0.0 147.1 jit_solution(5763729873363414824)
XLA Ops:
  6.5 0.7 all-gather.3.cloned.1.call-update
  8.0 1.0 copy.151
  9.0 1.0 copy.148
  10.1 11.5 %all_gather.26 = bf16[1024,64]{0,1:T(8,128)(2,1)S(1)} all-gather(bf16[256,64]{0,1:T(8,128)(2,1)} %param.29), channel_id=1, replica_groups=mesh['grp'=2,'sp'=4,'tp'=4] {'sp'}, dimensions={0}, use_global_device_ids=true | all-gather | bytes 163840 | tf_op jit(solution)/shard_map/all_gather | solution.py:205
  21.6 0.8 copy.178
  24.1 14.2 %all_gather.27 = bf16[1024,128]{1,0:T(8,128)(2,1)S(1)} all-gather(bf16[256,128]{1,0:T(8,128)(2,1)S(1)} %copy-done.2), channel_id=1, replica_groups=mesh['grp'=2,'sp'=4,'tp'=4] {'sp'}, dimensions={0}, use_global_device_ids=true | all-gather | bytes 327680 | tf_op jit(solution)/shard_map/all_gather | solution.py:207
  38.8 24.4 %while.52 = (s32[]{:T(128)}, f32[2,128,128]{2,1,0:T(8,128)S(1)}, f32[8,32,2,128]{3,1,0,2:T(8,128)S(1)}, f32[8,32,2,128]{3,2,1,0:T(2,128)S(1)}, f32[8,32,2,128]{3...) while((s32[]{:T(128)}, f32[2,128,128]{2,1,0:T(8,128)S(1)}, ...), condition=%wide.region_2.3_spmd.clone, body=%wide.region_0.2_spmd.clone.sunk | while | flops 30302212 | bytes 3405956 | solution.py:86
  39.0 1.2 multiply_bitcast_fusion.2
  42.1 1.2 multiply_bitcast_fusion.2
  45.1 1.2 multiply_bitcast_fusion.2
  48.2 1.2 multiply_bitcast_fusion.2
  51.2 1.2 multiply_bitcast_fusion.2
  54.3 1.2 multiply_bitcast_fusion.2
  57.4 1.2 multiply_bitcast_fusion.2
  60.4 1.2 multiply_bitcast_fusion.2
  63.3 10.6 %all_gather.28 = bf16[1024,64]{0,1:T(8,128)(2,1)S(1)} all-gather(bf16[256,64]{0,1:T(8,128)(2,1)S(1)} %copy-done.5), channel_id=1, replica_groups=mesh['grp'=2,'sp'=4,'tp'=4] {'sp'}, dimensions={0}, use_global_device_ids=true | all-gather | bytes 163840 | tf_op jit(solution)/shard_map/all_gather | solution.py:206
  74.4 4.8 %while.51 = (s32[]{:T(128)}, f32[1,2,256]{2,1,0:T(2,128)S(1)}, f32[1,2,256]{2,1,0:T(2,128)S(1)}, f32[1,2,256,128]{3,2,1,0:T(8,128)S(1)}, f32[1,2,256]{2,1,0:T(2,...) while((s32[]{:T(128)}, f32[1,2,256]{2,1,0:T(2,128)S(1)}, ...), condition=%wide.region_15.16_spmd.clone, body=%wide.region_8.15_spmd.clone.sunk | while | flops 206442240 | bytes 8724921 | solution.py:222
  74.4 2.3 %conditional.3 = (f32[1,2,256]{2,1,0:T(2,128)S(1)}, f32[1,2,256]{2,1,0:T(2,128)S(1)}, f32[1,2,256,128]{3,2,1,0:T(8,128)S(1)}, f32[1,2,256]{2,1,0:T(2,128)S(1)}, ...) conditional(s32[]{:T(128)} %convert_element_type.97, (s32[]{:T(128)}, s32[]{:T(128)}, ...), branch_computations={%region_9.13_spmd, %region_14.14_spmd} | conditional | flops 206442240 | bytes 8715370 | solution.py:197
  76.8 2.3 %conditional.3 = (f32[1,2,256]{2,1,0:T(2,128)S(1)}, f32[1,2,256]{2,1,0:T(2,128)S(1)}, f32[1,2,256,128]{3,2,1,0:T(8,128)S(1)}, f32[1,2,256]{2,1,0:T(2,128)S(1)}, ...) conditional(s32[]{:T(128)} %convert_element_type.97, (s32[]{:T(128)}, s32[]{:T(128)}, ...), branch_computations={%region_9.13_spmd, %region_14.14_spmd} | conditional | flops 206442240 | bytes 8715370 | solution.py:197
  79.6 5.6 %all_gather.22 = bf16[4,2,128]{2,1,0:T(2,128)(2,1)S(1)} all-gather(bf16[1,2,128]{2,1,0:T(2,128)(2,1)S(1)} %fusion.67), channel_id=1, replica_groups=mesh['grp'=2,'sp'=4,'tp'=4] {'sp'}, dimensions={0}, use_global_device_ids=true | all-gather | bytes 2560 | tf_op jit(solution)/shard_map/all_gather | solution.py:20
  85.2 11.2 %all-gather = bf16[8,128,128]{2,1,0:T(8,128)(2,1)S(1)} all-gather(bf16[2,128,128]{2,1,0:T(8,128)(2,1)S(1)} %convert_element_type.73), channel_id=2, replica_groups=mesh['grp'=2,'sp'=4,'tp'=4] {'sp'}, dimensions={0}, use_global_device_ids=true | all-gather | bytes 327680 | tf_op jit(solution)/shard_map/all_gather | solution.py:20
  98.3 1.8 %fusion.60 = f32[256,2048]{1,0:T(8,128)S(1)} fusion(bf16[256,256]{0,1:T(8,128)(2,1)S(1)} %bitcast.210, bf16[2,256,2048]{2,1,0:T(8,128)(2,1)} %all-gather.3.cloned.1.call-done), kind=kOutput, calls=%fused_computation.91 | convolution fusion | flops 268435456 | bytes 3276800 | tf_op jit(solution)/shard_map/dot_general | solution.py:268
  100.2 1.4 fusion.58
  101.7 38.6 %reduce-scatter.2.cloned.1.call-done = bf16[64,2048]{1,0:T(8,128)(2,1)} async-done(((bf16[256,2048]{1,0:T(8,128)(2,1)}), bf16[64,2048]{1,0:T(8,128)(2,1)}) %reduce-scatter.2.cloned.1.call-update) | async-done | bytes 262160 | tf_op jit(solution)/shard_map/reduce_scatter | solution.py:271
  (207 shorter events, 24.2 us)
Async XLA Ops:
  6.5 16.0 %copy-start.6 = (f32[256,2]{0,1:T(2,128)S(1)}, f32[256,2]{0,1:T(2,128)}, u32[]{:S(2)}) copy-start(f32[256,2]{0,1:T(2,128)} %param.26) | copy-start | bytes 6148
  6.5 91.7 %all-gather.3.cloned.1.call-start = ((), (), s32[]{:S(2)}) async-start(), calls=%async_computation.1 | async-start | bytes 2621440 | tf_op jit(solution)/shard_map/all_gather | solution.py:267
  7.3 133.0 %reduce-scatter.2.cloned.1.call-start = ((), (), s32[]{:S(2)}) async-start(), calls=%async_computation.2 | async-start | bytes 1310720 | tf_op jit(solution)/shard_map/reduce_scatter | solution.py:271
  22.8 1.2 copy-start.1
  22.9 1.2 copy-start.2
  38.8 24.5 %copy-start.5 = (bf16[256,64]{0,1:T(8,128)(2,1)S(1)}, bf16[256,64]{0,1:T(8,128)(2,1)}, u32[]{:S(2)}) copy-start(bf16[256,64]{0,1:T(8,128)(2,1)} %param.31) | copy-start | bytes 98308
  38.8 35.1 %copy-start.3 = (bf16[256,128]{1,0:T(8,128)(2,1)S(1)}, bf16[256,128]{1,0:T(8,128)(2,1)}, u32[]{:S(2)}) copy-start(bf16[256,128]{1,0:T(8,128)(2,1)} %param.28) | copy-start | bytes 196612
  38.8 35.2 %copy-start.4 = (bf16[256,128]{1,0:T(8,128)(2,1)S(1)}, bf16[256,128]{1,0:T(8,128)(2,1)}, u32[]{:S(2)}) copy-start(bf16[256,128]{1,0:T(8,128)(2,1)} %param.30) | copy-start | bytes 196612
  79.2 17.3 %copy-start.9 = (f32[2]{0:T(128)S(1)}, f32[2]{0:T(128)}, u32[]{:S(2)}) copy-start(f32[2]{0:T(128)} %param.33) | copy-start | bytes 28
  96.4 1.6 %copy-start.7 = (f32[128]{0:T(128)S(1)}, f32[128]{0:T(128)}, u32[]{:S(2)}) copy-start(f32[128]{0:T(128)} %param.34) | copy-start | bytes 1540
  96.5 1.6 %copy-start.8 = (f32[128]{0:T(128)S(1)}, f32[128]{0:T(128)}, u32[]{:S(2)}) copy-start(f32[128]{0:T(128)} %param.27) | copy-start | bytes 1540
  98.3 1.9 %copy-start = (bf16[2,256,2048]{2,1,0:T(8,128)(2,1)S(1)}, bf16[2,256,2048]{2,1,0:T(8,128)(2,1)}, u32[]{:S(2)}) copy-start(bf16[2,256,2048]{2,1,0:T(8,128)(2,1)} %all-gather.3.cloned.1.call-done) | copy-start | bytes 6291460
Sparse Core Ops, SparseCore 0:
  8.9 49.3 all-gather.2
  101.8 38.4 reduce-scatter.1
where the time goes:
time: 149 us; the launch traced here: 147 us
  blocking collectives  53.1 us (36%)
  waiting for transfers between devices  39.4 us (26%)
  other arithmetic  20.5 us (14%)
  matrix products  13.9 us (9%)
  between operations  13.9 us (9%)
  local copies, waits for them, and re-layouts  5.08 us (3%)
    reduce_scatter x1, waiting for transfers between devices, shards(): lax.psum_scatter(partial_terms.astype(jnp.bfloat16), 'tp', scatter_dimens...  38.6 us
    all_gather x2, blocking collectives, carried_in(): lax.all_gather(part.astype(kind), axis)  16.8 us
    all_gather x1, blocking collectives, attention_branch(): shard_values = lax.all_gather(attention_value, 'sp', axis=0, tiled=True)  14.2 us
    all_gather x1, blocking collectives, attention_branch(): shard_one = lax.all_gather(attention_key_first, 'sp', axis=0, tiled=True)  11.5 us
    all_gather x1, blocking collectives, attention_branch(): shard_two = lax.all_gather(attention_key_second, 'sp', axis=0, tiled=True)  10.6 us
    while x8, other arithmetic  9.95 us
    dot_general x8, other arithmetic, block_step(): jnp.einsum('thd,shd,tshd->hts', query_blk, inflow_blk, decay_table, preci...  5.64 us
    dot_general x8, matrix products, block_step(): jnp.einsum('shd,shv->hdv', inflow_blk * jnp.exp(last_log[None] - cumulati...  3.15 us
  transfers between devices with their start and end apart: 2, of which 1 were waited for; matrix products, arithmetic and copies ran while one was open for 25% of the time, Pallas kernels for 0%

commit v1 on v0

--- a/solution.py
+++ b/solution.py
@@ -1,6 +1,8 @@
 import jax
 import jax.numpy as jnp
 from jax import lax
+from jax.experimental import pallas as pl
+from jax.experimental.pallas import tpu as pltpu
 from jax.sharding import PartitionSpec as P
 
 HG_DK = 128
@@ -273,9 +275,374 @@
     )
 
 
+CHUNK = 64
+MESH = pl.DeviceIdType.MESH
+BF = jnp.bfloat16
+F32 = jnp.float32
+
+
+def nt(a, b):
+    return lax.dot_general(a, b, (((1,), (1,)), ((), ())), preferred_element_type=F32)
+
+
+def tn(a, b):
+    return lax.dot_general(a, b, (((0,), (0,)), ((), ())), preferred_element_type=F32)
+
+
+def nn(a, b):
+    return jnp.dot(a, b, preferred_element_type=F32)
+
+
+def layer_kernel(
+    G, S, T,
+    rq, fg, rv, lb, ad, rg, q1, k1, q2, k2, v, lam, ag, w,
+    out,
+    kv, wbuf, pbuf, rbuf, st_out, st_in, fst, rec, qrun, qs, m_ref, l_ref, acc, x,
+    kv_send, kv_recv, st_send, st_recv, up_send, dn_send, wz_recv, wy_send, wy_recv,
+    rs_send, rs_recv, loc,
+):
+    g, z, j = lax.axis_index("grp"), lax.axis_index("sp"), lax.axis_index("tp")
+    rows = rq.shape[0]
+    heads = rq.shape[1] // HG_DK
+    groups = q1.shape[1] // DA_HD
+    cols = w.shape[2]
+    share = rows // T
+    up, dn = z + 1, z - 1
+    has_up, has_dn = z + 1 < S, z > 0
+
+    own_w = pltpu.make_async_copy(w, wbuf.at[z], loc)
+    own_w.start()
+
+    lane = lax.broadcasted_iota(jnp.int32, (rows, 2 * DA_HD), 1)
+    kv[z, 0] = jnp.concatenate([k1[...], k2[...]], axis=1)
+    kv[z, 1] = v[...]
+
+    barrier = pltpu.get_barrier_semaphore()
+
+    @pl.when(has_up)
+    def _():
+        pl.semaphore_signal(barrier, inc=1, device_id={"sp": up}, device_id_type=MESH)
+
+    @pl.when(has_dn)
+    def _():
+        pl.semaphore_signal(barrier, inc=1, device_id={"sp": dn}, device_id_type=MESH)
+
+    if G == 2:
+        pl.semaphore_signal(barrier, inc=1, device_id={"grp": 1 - g}, device_id_type=MESH)
+    for o in range(1, T):
+        pl.semaphore_signal(
+            barrier, inc=1, device_id={"tp": lax.rem(j + o, T)}, device_id_type=MESH
+        )
+    pl.semaphore_wait(
+        barrier, jnp.where(has_up, 1, 0) + jnp.where(has_dn, 1, 0) + (G - 1) + (T - 1)
+    )
+
+    def kv_copy(k, slot):
+        return pltpu.make_async_remote_copy(
+            src_ref=kv.at[k], dst_ref=kv.at[k], send_sem=kv_send.at[slot],
+            recv_sem=kv_recv.at[k], device_id={"sp": up}, device_id_type=MESH)
+
+    def half(ref):
+        return ref.at[g] if G == 2 else ref
+
+    def w_copy(k, slot, upward):
+        source = half(w) if slot == 0 else half(wbuf.at[k])
+        return pltpu.make_async_remote_copy(
+            src_ref=source, dst_ref=half(wbuf.at[k]),
+            send_sem=(up_send if upward else dn_send).at[slot], recv_sem=wz_recv.at[k],
+            device_id={"sp": up if upward else dn}, device_id_type=MESH)
+
+    def y_copy(k, which):
+        return pltpu.make_async_remote_copy(
+            src_ref=wbuf.at[k, which], dst_ref=wbuf.at[k, which],
+            send_sem=wy_send.at[k], recv_sem=wy_recv.at[k],
+            device_id={"grp": 1 - g}, device_id_type=MESH)
+
+    def st_copy():
+        return pltpu.make_async_remote_copy(
+            src_ref=st_out, dst_ref=st_in, send_sem=st_send.at[0], recv_sem=st_recv.at[0],
+            device_id={"sp": up}, device_id_type=MESH)
+
+    def rs_copy(k, o):
+        to = lax.rem(j + o, T)
+        return pltpu.make_async_remote_copy(
+            src_ref=pbuf.at[k, to], dst_ref=rbuf.at[o, k],
+            send_sem=rs_send.at[k, o], recv_sem=rs_recv.at[k, o],
+            device_id={"tp": to}, device_id_type=MESH)
+
+    @pl.when(has_up)
+    def _():
+        kv_copy(z, 0).start()
+
+    @pl.when(has_dn)
+    def _():
+        w_copy(z, 0, False).start()
+
+    inflow = jax.nn.sigmoid(-lb[...]) * jax.nn.sigmoid(-fg[...].astype(F32))
+    added = jnp.concatenate(
+        [jnp.broadcast_to(ad[:, h : h + 1], (rows, HG_DK)) for h in range(heads)], axis=1
+    )
+    logd = jnp.log1p(-inflow) + added
+    hi = logd.astype(BF)
+    lo = (logd - hi.astype(F32)).astype(BF)
+    ti = lax.broadcasted_iota(jnp.int32, (rows, rows), 0)
+    si = lax.broadcasted_iota(jnp.int32, (rows, rows), 1)
+    tril = ti >= si
+    trib = jnp.where(tril, 1.0, 0.0).astype(BF)
+    blockb = jnp.where(tril & (ti // CHUNK == si // CHUNK), 1.0, 0.0).astype(BF)
+    cum = nn(blockb, hi) + nn(blockb, lo)
+    run = nn(trib, hi) + nn(trib, lo)
+    q = rq[...].astype(F32)
+    qd = (q * jnp.exp(cum)).astype(BF)
+    kd = (inflow * jnp.exp(-cum)).astype(BF)
+    qrun[...] = (q * jnp.exp(run)).astype(BF)
+    total = jnp.exp(run[rows - 1 : rows, :])
+    small = (
+        lax.broadcasted_iota(jnp.int32, (CHUNK, CHUNK), 0)
+        >= lax.broadcasted_iota(jnp.int32, (CHUNK, CHUNK), 1)
+    )
+    for h in range(heads):
+        cs = slice(h * HG_DK, (h + 1) * HG_DK)
+        state = None
+        for c in range(rows // CHUNK):
+            rs = slice(c * CHUNK, (c + 1) * CHUNK)
+            vc = rv[rs, cs]
+            sc = jnp.where(small, nt(qd[rs, cs], kd[rs, cs]), 0.0).astype(BF)
+            o = nn(sc, vc)
+            if state is not None:
+                o = o + nt(qd[rs, cs], state.astype(BF))
+            rec[rs, cs] = o
+            last = cum[(c + 1) * CHUNK - 1 : (c + 1) * CHUNK, cs]
+            kend = (inflow[rs, cs] * jnp.exp(last - cum[rs, cs])).astype(BF)
+            add = tn(vc, kend)
+            state = add if state is None else jnp.exp(last) * state + add
+        fst[h] = state
+
+    @pl.when(jnp.logical_and(z == 0, has_up))
+    def _():
+        st_out[...] = fst[...].astype(BF)
+        st_copy().start()
+
+    def kv_arrive(d):
+        @pl.when(z >= d)
+        def _():
+            kv_copy(z - d, 0).wait_recv()
+
+            @pl.when(has_up)
+            def _():
+                kv_copy(z - d, d).start()
+
+    q1f = q1[...].astype(F32) * (DA_HD ** -0.5)
+    q2f = q2[...].astype(F32) * (DA_HD ** -0.5)
+    low = lane < DA_HD
+    for h in range(groups):
+        a = jnp.concatenate([q1f[:, h * DA_HD : (h + 1) * DA_HD], jnp.zeros((rows, DA_HD), F32)], 1)
+        b = jnp.concatenate([jnp.zeros((rows, DA_HD), F32), q2f[:, h * DA_HD : (h + 1) * DA_HD]], 1)
+        qs[h] = a.astype(BF)
+        qs[groups + h] = b.astype(BF)
+
+    def attend(k, first):
+        for r in range(2 * groups):
+            s = nt(qs[r], kv[k, 0])
+            if first:
+                s = jnp.where(tril, s, -1e30)
+                top = jnp.max(s, axis=1, keepdims=True)
+            else:
+                top = jnp.maximum(m_ref[r], jnp.max(s, axis=1, keepdims=True))
+            p = jnp.exp(s - top)
+            mass = jnp.sum(p, axis=1, keepdims=True)
+            val = nn(p.astype(BF), kv[k, 1])
+            if not first:
+                shrink = jnp.exp(m_ref[r] - top)
+                mass = mass + l_ref[r] * shrink
+                val = val + acc[r] * shrink
+            m_ref[r] = top
+            l_ref[r] = mass
+            acc[r] = val
+
+    if S > 1:
+        kv_arrive(1)
+    attend(z, True)
+    if S > 2:
+        kv_arrive(2)
+
+    @pl.when(has_dn)
+    def _():
+        st_copy().wait_recv()
+
+        @pl.when(has_up)
+        def _():
+            for h in range(heads):
+                st_out[h] = (
+                    total[:, h * HG_DK : (h + 1) * HG_DK] * st_in[h].astype(F32) + fst[h]
+                ).astype(BF)
+            st_copy().start()
+
+        for h in range(heads):
+            cs = slice(h * HG_DK, (h + 1) * HG_DK)
+            rec[:, cs] = rec[:, cs] + nt(qrun[:, cs], st_in[h])
+
+    for d in range(3, S):
+        kv_arrive(d)
+
+    @pl.when(has_up)
+    def _():
+        w_copy(z, 0, True).start()
+
+    def w_arrive(d, upward):
+        k = z - d if upward else z + d
+        there = (z >= d) if upward else (z + d < S)
+        onward = has_up if upward else has_dn
+
+        @pl.when(there)
+        def _():
+            w_copy(k, 1, upward).wait_recv()
+
+            @pl.when(onward)
+            def _():
+                w_copy(k, d, upward).start()
+
+            if G == 2:
+                y_copy(k, g).start()
+
+    w_arrive(1, False)
+    for d in range(1, S):
+        @pl.when(z >= d)
+        def _(d=d):
+            attend(z - d, False)
+
+    for h in range(heads):
+        cs = slice(h * HG_DK, (h + 1) * HG_DK)
+        x[:, cs] = head_norm(rec[:, cs], rg[...]).astype(BF)
+    for h in range(groups):
+        mixed = acc[h] / l_ref[h] - lam[h] * (acc[groups + h] / l_ref[groups + h])
+        base = heads * HG_DK + h * 2 * DA_HD
+        x[:, base : base + 2 * DA_HD] = head_norm(mixed, ag[...]).astype(BF)
+
+    split = heads * HG_DK
+
+    def project(k):
+        part = nn(x[:, :split], wbuf[k, 0]) + nn(x[:, split:], wbuf[k, 1])
+        pbuf[k] = part.astype(BF).reshape(T, share, cols)
+        for o in range(1, T):
+            rs_copy(k, o).start()
+
+    own_w.wait()
+    project(z)
+
+    def finish(d, upward):
+        k = z - d if upward else z + d
+        there = (z >= d) if upward else (z + d < S)
+
+        @pl.when(there)
+        def _():
+            if G == 2:
+                y_copy(k, 1 - g).wait_recv()
+            project(k)
+
+    for d in range(1, S):
+        w_arrive(d, True)
+        if d > 1:
+            w_arrive(d, False)
+            finish(d - 1, True)
+            finish(d - 1, False)
+    finish(S - 1, True)
+    finish(S - 1, False)
+
+    def gather_piece(k, carry):
+        total_sum = pbuf[k, j].astype(F32)
+        for o in range(1, T):
+            rs_copy(k, o).wait_recv()
+            total_sum = total_sum + rbuf[o, k].astype(F32)
+        out[:, pl.ds(pl.multiple_of(k * cols, cols), cols)] = total_sum.astype(BF)
+        return carry
+
+    gather_piece(z, 0)
+    for d in range(1, S):
+        for upward in (True, False):
+            @pl.when((z >= d) if upward else (z + d < S))
+            def _(d=d, upward=upward):
+                gather_piece(z - d if upward else z + d, 0)
+
+    @pl.when(has_up)
+    def _():
+        st_copy().wait_send()
+
+    for d in range(S):
+        @pl.when(jnp.logical_and(z >= d, has_up))
+        def _(d=d):
+            kv_copy(z - d, d).wait_send()
+            w_copy(z - d, d, True).wait_send()
+
+        @pl.when(jnp.logical_and(z + d < S, has_dn))
+        def _(d=d):
+            w_copy(z + d, d, False).wait_send()
+
+    if G == 2:
+        for d in range(1, S):
+            y_copy(lax.rem(z + d, S), g).wait_send()
+
+    for k in range(S):
+        for o in range(1, T):
+            rs_copy(k, o).wait_send()
+
+
+def fused_shards(G, S, T):
+    def body(rq, fg, rv, lb, ad, rg, q1, k1, q2, k2, v, lam, ag, w):
+        rows, cols = rq.shape[0], w.shape[2]
+        heads, groups = rq.shape[1] // HG_DK, q1.shape[1] // DA_HD
+        vm = pl.BlockSpec(memory_space=pltpu.VMEM)
+        specs = [vm] * 14
+        specs[11] = pl.BlockSpec(memory_space=pltpu.SMEM)
+        specs[13] = pl.BlockSpec(memory_space=pl.ANY)
+        dma = pltpu.SemaphoreType.DMA
+        return pl.pallas_call(
+            lambda *refs: layer_kernel(G, S, T, *refs),
+            out_shape=jax.ShapeDtypeStruct((rows // T, cols * S), BF),
+            in_specs=specs,
+            out_specs=vm,
+            scratch_shapes=[
+                pltpu.VMEM((S, 2, rows, 2 * DA_HD), BF),
+                pltpu.VMEM((S, 2, w.shape[1], cols), BF),
+                pltpu.VMEM((S, T, rows // T, cols), BF),
+                pltpu.VMEM((T, S, rows // T, cols), BF),
+                pltpu.VMEM((heads, HG_DV, HG_DK), BF),
+                pltpu.VMEM((heads, HG_DV, HG_DK), BF),
+                pltpu.VMEM((heads, HG_DV, HG_DK), F32),
+                pltpu.VMEM((rows, heads * HG_DV), F32),
+                pltpu.VMEM((rows, heads * HG_DK), BF),
+                pltpu.VMEM((2 * groups, rows, 2 * DA_HD), BF),
+                pltpu.VMEM((2 * groups, rows, 1), F32),
+                pltpu.VMEM((2 * groups, rows, 1), F32),
+                pltpu.VMEM((2 * groups, rows, 2 * DA_HD), F32),
+                pltpu.VMEM((rows, heads * HG_DV + groups * 2 * DA_HD), BF),
+                dma((S,)), dma((S,)), dma((1,)), dma((1,)), dma((S,)), dma((S,)), dma((S,)),
+                dma((S,)), dma((S,)), dma((S, T)), dma((S, T)), dma,
+            ],
+            compiler_params=pltpu.CompilerParams(collective_id=0, has_side_effects=True),
+            name="layer",
+        )(
+            rq, fg, rv, lb.reshape(1, -1), ad, rg.reshape(1, -1),
+            q1, k1, q2, k2, v, lam, ag.reshape(1, -1), w,
+        )
+
+    return body
+
+
+def pick(G, S, T):
+    def body(*args):
+        rows, cols = args[0].shape[0], args[13].shape[2]
+        one_key_head = args[7].shape[1] == DA_HD
+        if cols % 128 or not one_key_head or S < 2 or G > 2 or rows % (T * 16) or S > 16:
+            return shards(*args)
+        return fused_shards(G, S, T)(*args)
+
+    return body
+
+
 def solution(mesh):
     return jax.shard_map(
-        shards,
+        pick(mesh.shape["grp"], mesh.shape["sp"], mesh.shape["tp"]),
         mesh=mesh,
         in_specs=(
             P(("grp", "sp"), "tp"),

time: 149 us -> 50.7 us (0.34); the launches traced: 147 us -> 50.5 us
  blocking collectives: 53.1 us -> 0 us
  Pallas kernels: 0 us -> 45.8 us
  waiting for transfers between devices: 39.4 us -> 0 us
  other arithmetic: 20.5 us -> 0 us
  matrix products: 13.9 us -> 0 us
  between operations: 13.9 us -> 0.01 us
    all_gather x5 -> x0, blocking collectives: 53.1 us -> none  [the longest x2 16.8 us: carried_in(): lax.all_gather(part.astype(kind), axis)]
    pallas_call x0 -> x1, Pallas kernels: none -> 45.8 us  [body(): pl.pallas_call(lambda *refs: layer_kernel(G, S, T, *refs), out_shape=jax....]
    reduce_scatter x1 -> x0, waiting for transfers between devices: 38.6 us -> none  [shards(): lax.psum_scatter(partial_terms.astype(jnp.bfloat16), 'tp', scatter_dimens...]
    dot_general x35 -> x0, matrix products: 13.9 us -> none  [the longest x8 3.15 us: block_step(): jnp.einsum('shd,shv->hdv', inflow_blk * jnp.exp(last_log[None] - cumulati...]
    while x8 -> x0, other arithmetic: 9.95 us -> none
    dot_general x8 -> x0, other arithmetic: 5.64 us -> none  [block_step(): jnp.einsum('thd,shd,tshd->hts', query_blk, inflow_blk, decay_table, preci...]
    unnamed x24 -> x8, local copies, waits for them, and re-layouts: 2.35 us -> 4.7 us
  transfers between devices with their start and end apart: 2 -> 0, of which waited for: 1 -> 0; matrix products, arithmetic and copies ran while one was open for 25% -> 0% of each run, Pallas kernels for 0% -> 0%
where the time goes in v1:
time: 50.7 us; the launch traced here: 50.5 us
  Pallas kernels  45.8 us (90%)
  local copies, waits for them, and re-layouts  4.7 us (9%)
    pallas_call x1, Pallas kernels, body(): pl.pallas_call(lambda *refs: layer_kernel(G, S, T, *refs), out_shape=jax....  45.8 us
    unnamed x8, local copies, waits for them, and re-layouts  4.7 us

profile of v1, /device:TPU:25, one launch (start us, length us, event | category | flops | bytes accessed | tf_op | source)
XLA Modules:
  0.0 50.5 jit_solution(16317242564674617155)
XLA Ops:
  0.0 0.0 copy-start
  0.0 1.5 %copy.16.refs_7_ = bf16[256,64]{1,0:T(8,128)(2,1)} copy(bf16[256,64]{0,1:T(8,128)(2,1)} %param.21) | data formatting | bytes 65536 | tf_op args[7]
  1.5 0.0 copy-done
  1.5 0.0 copy-start.1
  1.5 0.7 %copy.17.refs_9_ = bf16[256,64]{1,0:T(8,128)(2,1)} copy(bf16[256,64]{0,1:T(8,128)(2,1)S(1)} %copy-done) | data formatting | bytes 65536 | tf_op args[9]
  2.2 0.0 copy-done.1
  2.2 0.8 %copy.15.refs_4_ = f32[256,2]{1,0:T(8,128)} copy(f32[256,2]{0,1:T(2,128)S(1)} %copy-done.1) | data formatting | bytes 4096 | tf_op args[4]
  3.0 45.8 %layer.1 = bf16[64,2048]{1,0:T(8,128)(2,1)} custom-call(bf16[256,256]{1,0:T(8,128)(2,1)} %refs_0_.1, bf16[256,256]{1,0:T(8,128)(2,1)} %refs_1_.1, bf16[256,256]{1,0:T(8,128)(2,1)} %refs_2_.1, f32[1,256]{1,0:T(1,128)} %bitcast.3, f32[256,2]{1,0:T(8,128)} %copy.15.refs_4_, f32[1,128]{1,0:T(1,128)} %bitcast.4, bf16[256,128]{1,0:T(8,128)(2,1)} %refs_6_.1, ...), custom_call_target="tpu_custom_call" | custom-call | tf_op jit(solution)/shard_map/layer/pallas_call | solution.py:599
  48.8 1.7 %copy.19 = bf16[64,2048]{1,0:T(8,128)(2,1)} copy(bf16[64,2048]{1,0:T(8,128)(2,1)} %layer.1) | data formatting | bytes 524288
Async XLA Ops:
  0.0 1.5 %copy-start = (bf16[256,64]{0,1:T(8,128)(2,1)S(1)}, bf16[256,64]{0,1:T(8,128)(2,1)}, u32[]{:S(2)}) copy-start(bf16[256,64]{0,1:T(8,128)(2,1)} %param.23) | copy-start | bytes 98308
  1.5 0.7 %copy-start.1 = (f32[256,2]{0,1:T(2,128)S(1)}, f32[256,2]{0,1:T(2,128)}, u32[]{:S(2)}) copy-start(f32[256,2]{0,1:T(2,128)} %param.18) | copy-start | bytes 6148

commit v2 on v1

--- a/solution.py
+++ b/solution.py
@@ -276,6 +276,7 @@
 
 
 CHUNK = 64
+PARTS = 2
 MESH = pl.DeviceIdType.MESH
 BF = jnp.bfloat16
 F32 = jnp.float32
@@ -297,7 +298,7 @@
     G, S, T,
     rq, fg, rv, lb, ad, rg, q1, k1, q2, k2, v, lam, ag, w,
     out,
-    kv, wbuf, pbuf, rbuf, st_out, st_in, fst, rec, qrun, qs, m_ref, l_ref, acc, x,
+    kt, vv, wbuf, pbuf, rbuf, st_out, st_in, fst, rec, qrun, qs, m_ref, l_ref, acc, x,
     kv_send, kv_recv, st_send, st_recv, up_send, dn_send, wz_recv, wy_send, wy_recv,
     rs_send, rs_recv, loc,
 ):
@@ -305,17 +306,21 @@
     rows = rq.shape[0]
     heads = rq.shape[1] // HG_DK
     groups = q1.shape[1] // DA_HD
-    cols = w.shape[2]
+    cols = w.shape[2] // PARTS
     share = rows // T
     up, dn = z + 1, z - 1
     has_up, has_dn = z + 1 < S, z > 0
 
-    own_w = pltpu.make_async_copy(w, wbuf.at[z], loc)
-    own_w.start()
-
-    lane = lax.broadcasted_iota(jnp.int32, (rows, 2 * DA_HD), 1)
-    kv[z, 0] = jnp.concatenate([k1[...], k2[...]], axis=1)
-    kv[z, 1] = v[...]
+    own_w = [
+        pltpu.make_async_copy(w.at[:, :, pl.ds(c * cols, cols)], wbuf.at[z, c], loc.at[c])
+        for c in range(PARTS)
+    ]
+    for one in own_w:
+        one.start()
+
+    kt[z, :DA_HD] = k1[...]
+    kt[z, DA_HD:] = k2[...]
+    vv[z] = v[...]
 
     barrier = pltpu.get_barrier_semaphore()
 
@@ -337,25 +342,26 @@
         barrier, jnp.where(has_up, 1, 0) + jnp.where(has_dn, 1, 0) + (G - 1) + (T - 1)
     )
 
-    def kv_copy(k, slot):
+    def kv_copies(k, slot):
+        return [
+            pltpu.make_async_remote_copy(
+                src_ref=ref.at[k], dst_ref=ref.at[k], send_sem=kv_send.at[slot, i],
+                recv_sem=kv_recv.at[k, i], device_id={"sp": up}, device_id_type=MESH)
+            for i, ref in enumerate((kt, vv))
+        ]
+
+    def w_copy(k, c, slot, upward):
+        mine = g if G == 2 else slice(None)
+        source = w.at[mine, :, pl.ds(c * cols, cols)] if slot == 0 else wbuf.at[k, c, mine]
         return pltpu.make_async_remote_copy(
-            src_ref=kv.at[k], dst_ref=kv.at[k], send_sem=kv_send.at[slot],
-            recv_sem=kv_recv.at[k], device_id={"sp": up}, device_id_type=MESH)
-
-    def half(ref):
-        return ref.at[g] if G == 2 else ref
-
-    def w_copy(k, slot, upward):
-        source = half(w) if slot == 0 else half(wbuf.at[k])
+            src_ref=source, dst_ref=wbuf.at[k, c, mine],
+            send_sem=(up_send if upward else dn_send).at[slot, c], recv_sem=wz_recv.at[k, c],
+            device_id={"sp": up if upward else dn}, device_id_type=MESH)
+
+    def y_copy(k, c, which):
         return pltpu.make_async_remote_copy(
-            src_ref=source, dst_ref=half(wbuf.at[k]),
-            send_sem=(up_send if upward else dn_send).at[slot], recv_sem=wz_recv.at[k],
-            device_id={"sp": up if upward else dn}, device_id_type=MESH)
-
-    def y_copy(k, which):
-        return pltpu.make_async_remote_copy(
-            src_ref=wbuf.at[k, which], dst_ref=wbuf.at[k, which],
-            send_sem=wy_send.at[k], recv_sem=wy_recv.at[k],
+            src_ref=wbuf.at[k, c, which], dst_ref=wbuf.at[k, c, which],
+            send_sem=wy_send.at[k, c], recv_sem=wy_recv.at[k, c],
             device_id={"grp": 1 - g}, device_id_type=MESH)
 
     def st_copy():
@@ -363,24 +369,27 @@
             src_ref=st_out, dst_ref=st_in, send_sem=st_send.at[0], recv_sem=st_recv.at[0],
             device_id={"sp": up}, device_id_type=MESH)
 
-    def rs_copy(k, o):
+    def rs_copy(k, c, o):
         to = lax.rem(j + o, T)
         return pltpu.make_async_remote_copy(
-            src_ref=pbuf.at[k, to], dst_ref=rbuf.at[o, k],
-            send_sem=rs_send.at[k, o], recv_sem=rs_recv.at[k, o],
+            src_ref=pbuf.at[k, c, to], dst_ref=rbuf.at[o, k, c],
+            send_sem=rs_send.at[k, c, o], recv_sem=rs_recv.at[k, c, o],
             device_id={"tp": to}, device_id_type=MESH)
 
     @pl.when(has_up)
     def _():
-        kv_copy(z, 0).start()
+        for one in kv_copies(z, 0):
+            one.start()
+        w_copy(z, 0, 0, True).start()
 
     @pl.when(has_dn)
     def _():
-        w_copy(z, 0, False).start()
+        for c in range(PARTS):
+            w_copy(z, c, 0, False).start()
 
     inflow = jax.nn.sigmoid(-lb[...]) * jax.nn.sigmoid(-fg[...].astype(F32))
     added = jnp.concatenate(
-        [jnp.broadcast_to(ad[:, h : h + 1], (rows, HG_DK)) for h in range(heads)], axis=1
+        [jnp.broadcast_to(ad[h : h + 1, :], (HG_DK, rows)).T for h in range(heads)], axis=1
     )
     logd = jnp.log1p(-inflow) + added
     hi = logd.astype(BF)
@@ -426,15 +435,34 @@
     def kv_arrive(d):
         @pl.when(z >= d)
         def _():
-            kv_copy(z - d, 0).wait_recv()
+            for one in kv_copies(z - d, 0):
+                one.wait_recv()
 
             @pl.when(has_up)
             def _():
-                kv_copy(z - d, d).start()
+                for one in kv_copies(z - d, d):
+                    one.start()
+
+    def w_arrive(d, c, upward):
+        if d >= S:
+            return
+        k = z - d if upward else z + d
+        there = (z >= d) if upward else (z + d < S)
+        onward = has_up if upward else has_dn
+
+        @pl.when(there)
+        def _():
+            w_copy(k, c, 1, upward).wait_recv()
+
+            @pl.when(onward)
+            def _():
+                w_copy(k, c, d, upward).start()
+
+            if G == 2:
+                y_copy(k, c, g).start()
 
     q1f = q1[...].astype(F32) * (DA_HD ** -0.5)
     q2f = q2[...].astype(F32) * (DA_HD ** -0.5)
-    low = lane < DA_HD
     for h in range(groups):
         a = jnp.concatenate([q1f[:, h * DA_HD : (h + 1) * DA_HD], jnp.zeros((rows, DA_HD), F32)], 1)
         b = jnp.concatenate([jnp.zeros((rows, DA_HD), F32), q2f[:, h * DA_HD : (h + 1) * DA_HD]], 1)
@@ -443,7 +471,7 @@
 
     def attend(k, first):
         for r in range(2 * groups):
-            s = nt(qs[r], kv[k, 0])
+            s = nn(qs[r], kt[k])
             if first:
                 s = jnp.where(tril, s, -1e30)
                 top = jnp.max(s, axis=1, keepdims=True)
@@ -451,7 +479,7 @@
                 top = jnp.maximum(m_ref[r], jnp.max(s, axis=1, keepdims=True))
             p = jnp.exp(s - top)
             mass = jnp.sum(p, axis=1, keepdims=True)
-            val = nn(p.astype(BF), kv[k, 1])
+            val = nn(p.astype(BF), vv[k])
             if not first:
                 shrink = jnp.exp(m_ref[r] - top)
                 mass = mass + l_ref[r] * shrink
@@ -460,8 +488,8 @@
             l_ref[r] = mass
             acc[r] = val
 
-    if S > 1:
-        kv_arrive(1)
+    kv_arrive(1)
+    w_arrive(1, 0, False)
     attend(z, True)
     if S > 2:
         kv_arrive(2)
@@ -478,38 +506,32 @@
                 ).astype(BF)
             st_copy().start()
 
+    @pl.when(has_up)
+    def _():
+        for c in range(1, PARTS):
+            w_copy(z, c, 0, True).start()
+
+    for c in range(1, PARTS):
+        w_arrive(1, c, False)
+    for d in range(3, S):
+        kv_arrive(d)
+    for d in range(1, S):
+        w_arrive(1 + d, 0, False)
+
+        @pl.when(z >= d)
+        def _(d=d):
+            attend(z - d, False)
+
+        if d == 1:
+            w_arrive(1, 0, True)
+        for c in range(1, PARTS):
+            w_arrive(1 + d, c, False)
+
+    @pl.when(has_dn)
+    def _():
         for h in range(heads):
             cs = slice(h * HG_DK, (h + 1) * HG_DK)
             rec[:, cs] = rec[:, cs] + nt(qrun[:, cs], st_in[h])
-
-    for d in range(3, S):
-        kv_arrive(d)
-
-    @pl.when(has_up)
-    def _():
-        w_copy(z, 0, True).start()
-
-    def w_arrive(d, upward):
-        k = z - d if upward else z + d
-        there = (z >= d) if upward else (z + d < S)
-        onward = has_up if upward else has_dn
-
-        @pl.when(there)
-        def _():
-            w_copy(k, 1, upward).wait_recv()
-
-            @pl.when(onward)
-            def _():
-                w_copy(k, d, upward).start()
-
-            if G == 2:
-                y_copy(k, g).start()
-
-    w_arrive(1, False)
-    for d in range(1, S):
-        @pl.when(z >= d)
-        def _(d=d):
-            attend(z - d, False)
 
     for h in range(heads):
         cs = slice(h * HG_DK, (h + 1) * HG_DK)
@@ -521,48 +543,48 @@
 
     split = heads * HG_DK
 
-    def project(k):
-        part = nn(x[:, :split], wbuf[k, 0]) + nn(x[:, split:], wbuf[k, 1])
-        pbuf[k] = part.astype(BF).reshape(T, share, cols)
+    def project(k, c):
+        part = nn(x[:, :split], wbuf[k, c, 0]) + nn(x[:, split:], wbuf[k, c, 1])
+        pbuf[k, c] = part.astype(BF).reshape(T, share, cols)
         for o in range(1, T):
-            rs_copy(k, o).start()
-
-    own_w.wait()
-    project(z)
-
-    def finish(d, upward):
+            rs_copy(k, c, o).start()
+
+    def finish(d, c, upward):
         k = z - d if upward else z + d
-        there = (z >= d) if upward else (z + d < S)
-
-        @pl.when(there)
+
+        @pl.when((z >= d) if upward else (z + d < S))
         def _():
             if G == 2:
-                y_copy(k, 1 - g).wait_recv()
-            project(k)
-
+                y_copy(k, c, 1 - g).wait_recv()
+            project(k, c)
+
+    for c in range(1, PARTS):
+        w_arrive(1, c, True)
+    for c in range(PARTS):
+        own_w[c].wait()
+        project(z, c)
+    for d in range(2, S + 1):
+        for c in range(PARTS):
+            w_arrive(d, c, True)
+        for c in range(PARTS):
+            finish(d - 1, c, False)
+            finish(d - 1, c, True)
+
+    def gather_piece(k):
+        for c in range(PARTS):
+            total_sum = pbuf[k, c, j].astype(F32)
+            for o in range(1, T):
+                rs_copy(k, c, o).wait_recv()
+                total_sum = total_sum + rbuf[o, k, c].astype(F32)
+            at = pl.multiple_of((k * PARTS + c) * cols, cols)
+            out[:, pl.ds(at, cols)] = total_sum.astype(BF)
+
+    gather_piece(z)
     for d in range(1, S):
-        w_arrive(d, True)
-        if d > 1:
-            w_arrive(d, False)
-            finish(d - 1, True)
-            finish(d - 1, False)
-    finish(S - 1, True)
-    finish(S - 1, False)
-
-    def gather_piece(k, carry):
-        total_sum = pbuf[k, j].astype(F32)
-        for o in range(1, T):
-            rs_copy(k, o).wait_recv()
-            total_sum = total_sum + rbuf[o, k].astype(F32)
-        out[:, pl.ds(pl.multiple_of(k * cols, cols), cols)] = total_sum.astype(BF)
-        return carry
-
-    gather_piece(z, 0)
-    for d in range(1, S):
-        for upward in (True, False):
+        for upward in (False, True):
             @pl.when((z >= d) if upward else (z + d < S))
             def _(d=d, upward=upward):
-                gather_piece(z - d if upward else z + d, 0)
+                gather_piece(z - d if upward else z + d)
 
     @pl.when(has_up)
     def _():
@@ -571,25 +593,28 @@
     for d in range(S):
         @pl.when(jnp.logical_and(z >= d, has_up))
         def _(d=d):
-            kv_copy(z - d, d).wait_send()
-            w_copy(z - d, d, True).wait_send()
+            for one in kv_copies(z - d, d):
+                one.wait_send()
+            for c in range(PARTS):
+                w_copy(z - d, c, d, True).wait_send()
 
         @pl.when(jnp.logical_and(z + d < S, has_dn))
         def _(d=d):
-            w_copy(z + d, d, False).wait_send()
-
-    if G == 2:
-        for d in range(1, S):
-            y_copy(lax.rem(z + d, S), g).wait_send()
-
-    for k in range(S):
-        for o in range(1, T):
-            rs_copy(k, o).wait_send()
+            for c in range(PARTS):
+                w_copy(z + d, c, d, False).wait_send()
+
+    for c in range(PARTS):
+        if G == 2:
+            for d in range(1, S):
+                y_copy(lax.rem(z + d, S), c, g).wait_send()
+        for k in range(S):
+            for o in range(1, T):
+                rs_copy(k, c, o).wait_send()
 
 
 def fused_shards(G, S, T):
     def body(rq, fg, rv, lb, ad, rg, q1, k1, q2, k2, v, lam, ag, w):
-        rows, cols = rq.shape[0], w.shape[2]
+        rows, cols = rq.shape[0], w.shape[2] // PARTS
         heads, groups = rq.shape[1] // HG_DK, q1.shape[1] // DA_HD
         vm = pl.BlockSpec(memory_space=pltpu.VMEM)
         specs = [vm] * 14
@@ -598,14 +623,15 @@
         dma = pltpu.SemaphoreType.DMA
         return pl.pallas_call(
             lambda *refs: layer_kernel(G, S, T, *refs),
-            out_shape=jax.ShapeDtypeStruct((rows // T, cols * S), BF),
+            out_shape=jax.ShapeDtypeStruct((rows // T, w.shape[2] * S), BF),
             in_specs=specs,
             out_specs=vm,
             scratch_shapes=[
-                pltpu.VMEM((S, 2, rows, 2 * DA_HD), BF),
-                pltpu.VMEM((S, 2, w.shape[1], cols), BF),
-                pltpu.VMEM((S, T, rows // T, cols), BF),
-                pltpu.VMEM((T, S, rows // T, cols), BF),
+                pltpu.VMEM((S, 2 * DA_HD, rows), BF),
+                pltpu.VMEM((S, rows, 2 * DA_HD), BF),
+                pltpu.VMEM((S, PARTS, 2, w.shape[1], cols), BF),
+                pltpu.VMEM((S, PARTS, T, rows // T, cols), BF),
+                pltpu.VMEM((T, S, PARTS, rows // T, cols), BF),
                 pltpu.VMEM((heads, HG_DV, HG_DK), BF),
                 pltpu.VMEM((heads, HG_DV, HG_DK), BF),
                 pltpu.VMEM((heads, HG_DV, HG_DK), F32),
@@ -616,14 +642,15 @@
                 pltpu.VMEM((2 * groups, rows, 1), F32),
                 pltpu.VMEM((2 * groups, rows, 2 * DA_HD), F32),
                 pltpu.VMEM((rows, heads * HG_DV + groups * 2 * DA_HD), BF),
-                dma((S,)), dma((S,)), dma((1,)), dma((1,)), dma((S,)), dma((S,)), dma((S,)),
-                dma((S,)), dma((S,)), dma((S, T)), dma((S, T)), dma,
+                dma((S, 2)), dma((S, 2)), dma((1,)), dma((1,)), dma((S, PARTS)), dma((S, PARTS)),
+                dma((S, PARTS)), dma((S, PARTS)), dma((S, PARTS)), dma((S, PARTS, T)),
+                dma((S, PARTS, T)), dma((PARTS,)),
             ],
             compiler_params=pltpu.CompilerParams(collective_id=0, has_side_effects=True),
             name="layer",
         )(
-            rq, fg, rv, lb.reshape(1, -1), ad, rg.reshape(1, -1),
-            q1, k1, q2, k2, v, lam, ag.reshape(1, -1), w,
+            rq, fg, rv, lb.reshape(1, -1), ad.T, rg.reshape(1, -1),
+            q1, k1.T, q2, k2.T, v, lam, ag.reshape(1, -1), w,
         )
 
     return body
@@ -633,7 +660,7 @@
     def body(*args):
         rows, cols = args[0].shape[0], args[13].shape[2]
         one_key_head = args[7].shape[1] == DA_HD
-        if cols % 128 or not one_key_head or S < 2 or G > 2 or rows % (T * 16) or S > 16:
+        if cols % (128 * PARTS) or not one_key_head or S < 2 or G > 2 or rows % (T * 16) or S > 16:
             return shards(*args)
         return fused_shards(G, S, T)(*args)
 

time: 50.7 us -> 46.5 us (0.917)
  local copies, waits for them, and re-layouts: 4.7 us -> 1.67 us
  Pallas kernels: 45.8 us -> 44.5 us
    unnamed x8 -> x1, local copies, waits for them, and re-layouts: 4.7 us -> 1.67 us
    pallas_call x1, Pallas kernels: 45.8 us -> 44.5 us  [body(): pl.pallas_call(lambda *refs: layer_kernel(G, S, T, *refs), out_shape=jax....]
where the time goes in v2:
time: 46.5 us; the launch traced here: 46.1 us
  Pallas kernels  44.5 us (96%)
  local copies, waits for them, and re-layouts  1.67 us (4%)
    pallas_call x1, Pallas kernels, body(): pl.pallas_call(lambda *refs: layer_kernel(G, S, T, *refs), out_shape=jax....  44.5 us
    unnamed x1, local copies, waits for them, and re-layouts  1.67 us

profile of v2, /device:TPU:25, one launch (start us, length us, event | category | flops | bytes accessed | tf_op | source)
XLA Modules:
  0.0 46.1 jit_solution(2188811813386609490)
XLA Ops:
  0.0 44.5 %layer.1 = bf16[64,2048]{1,0:T(8,128)(2,1)} custom-call(bf16[256,256]{1,0:T(8,128)(2,1)} %refs_0_.1, bf16[256,256]{1,0:T(8,128)(2,1)} %refs_1_.1, bf16[256,256]{1,0:T(8,128)(2,1)} %refs_2_.1, f32[1,256]{1,0:T(1,128)} %bitcast.9, f32[2,256]{1,0:T(2,128)} %bitcast.8, f32[1,128]{1,0:T(1,128)} %bitcast.10, bf16[256,128]{1,0:T(8,128)(2,1)} %refs_6_.1, ...), custom_call_target="tpu_custom_call" | custom-call | tf_op jit(solution)/shard_map/layer/pallas_call | solution.py:624
  44.5 1.7 %copy.16 = bf16[64,2048]{1,0:T(8,128)(2,1)} copy(bf16[64,2048]{1,0:T(8,128)(2,1)} %layer.1) | data formatting | bytes 524288
